TPU v7x, 512 devices: a whole 4x4x16 slice. The times are simulated.
512 devices in a mesh: ep: 32 (over z, core), tp: 16 (over y, x).
Axes of the slice: x: 4, y: 4, z: 16, core: 2. Of those that a mesh axis runs over, the one named last changes fastest.
Arguments:
- tokens: bfloat16 [4096, 2048], P('ep'), may hold values from -6 to 6
- selected: int32 [32, 1024], P(None, 'ep'), may hold values from -1 to 127, as said below
- affinity: float32 [32, 1024], P(None, 'ep'), may hold values from 0.05 to 1
- w_gate: bfloat16 [32, 2048, 2048], P('ep', None, 'tp'), may hold values from -0.125 to 0.125
- w_up: bfloat16 [32, 2048, 2048], P('ep', None, 'tp'), may hold values from -0.125 to 0.125
- w_down: bfloat16 [32, 2048, 2048], P('ep', 'tp'), may hold values from -0.125 to 0.125
Outputs:
- combined: bfloat16 [4096, 2048], P('ep', 'tp')
Inputs may be any that keep to these rules, and one draw needn't show every extreme that they name: `selected`: row e holds 32 aligned groups of 32 entries; the live entries of group j are distinct positions within the j-th block of 128 tokens, stand at the front of the group and are followed by -1; each row has 512 live entries in all, the number in a group varies, and some group of every row is full.
All inputs are finite; a program needn't handle non-finite values.
Results may differ from a plain program's by a relative error of at most 0.015.
Values may be sent and summed in bfloat16 or wider, within the bound.
A program may use at most 64 MiB of HBM per device.

v0:
```python
import jax
import jax.numpy as jnp
from jax import lax
from jax.sharding import Mesh
from jax.sharding import PartitionSpec as P

EP = ("ep_0", "ep_1")


def in_blocks(array, dim, peers):
    dims = array.shape
    parts = array.reshape(*dims[:dim], peers, dims[dim] // peers, *dims[dim + 1 :])
    return jnp.moveaxis(parts, dim, 0)


def joined_along(parts, dim):
    dims = list(parts.shape[1:])
    dims[dim] *= parts.shape[0]
    return jnp.moveaxis(parts, 0, dim).reshape(dims)


def moved_by_axis(parts, axes, order):
    dims = [lax.axis_size(a) for a in axes]
    parts = parts.reshape(*dims, *parts.shape[1:])
    for k in order:
        parts = lax.all_to_all(parts, axes[k], split_axis=k, concat_axis=k, tiled=True)
    return parts.reshape(-1, *parts.shape[len(axes) :])


def two_step_exchange(array, groups, order, split_dim, concat_dim):
    peers = lax.axis_size(groups[0]) * lax.axis_size(groups[1])
    parts = in_blocks(array, split_dim, peers)
    return joined_along(moved_by_axis(parts, groups, order), concat_dim)


def sent_to_all(array, axis):
    peers = lax.axis_size(axis)
    return lax.all_to_all(
        jnp.broadcast_to(array[None], (peers, *array.shape)), axis, 0, 0, tiled=True
    )


def gather_directly(array, axis, dim):
    parts = sent_to_all(array, axis)
    return joined_along(parts, dim)


def summed_on_arrival(array, axis, dim):
    peers = lax.axis_size(axis)
    parts = lax.all_to_all(in_blocks(array, dim, peers), axis, 0, 0, tiled=True)
    return jnp.sum(parts.astype(jnp.float32), axis=0)


def per_device(tokens, selected, affinity, w_gate, w_up, w_down):
    ep_count = lax.axis_size(EP)
    tp_count = lax.axis_size("tp")
    local_tokens = tokens.shape[0]
    width = tokens.shape[1]
    experts_here = w_gate.shape[0]
    slot_count = selected.shape[1]
    clamped = jnp.maximum(selected, 0)
    gathered = jnp.take(tokens, clamped, axis=0)
    column_span = width // tp_count
    slab = lax.dynamic_slice_in_dim(gathered, lax.axis_index("tp") * column_span, column_span, 2)
    arrived = two_step_exchange(slab, ("ep_0", "ep_1"), (1, 0), 0, 1)
    segment = gather_directly(arrived, "tp", 2)
    gate_more = jnp.einsum("ecd,edf->ecf", segment, w_gate, preferred_element_type=jnp.float32)
    up_more = jnp.einsum("ecd,edf->ecf", segment, w_up, preferred_element_type=jnp.float32)
    hidden = (jax.nn.silu(gate_more) * up_more).astype(jnp.bfloat16)
    summed = summed_on_arrival(
        jnp.einsum("efd,ecf->dec", w_down, hidden, preferred_element_type=jnp.float32).astype(
            jnp.bfloat16
        ),
        "tp",
        0,
    ).astype(jnp.bfloat16)
    summed = summed.reshape(summed.shape[0], experts_here, ep_count, slot_count)
    returned = lax.all_to_all(summed, EP, split_axis=2, concat_axis=1, tiled=True)
    feature_cols = returned.shape[0]
    returned = returned.reshape(feature_cols, experts_here * ep_count * slot_count)
    weights = jnp.where(selected >= 0, affinity, jnp.zeros_like(affinity)).reshape(-1)
    scaled_rows = returned.astype(jnp.float32).T * weights[:, None]
    combined = (
        jnp.zeros((local_tokens, feature_cols), jnp.float32)
        .at[clamped.reshape(-1)]
        .add(scaled_rows)
    )
    return combined.astype(jnp.bfloat16)


def solution(mesh):
    torus = Mesh(mesh.devices.reshape(16, 2, mesh.shape["tp"]), ("ep_0", "ep_1", "tp"))
    in_specs = (
        P(EP, None),
        P(None, EP),
        P(None, EP),
        P(EP, None, "tp"),
        P(EP, None, "tp"),
        P(EP, "tp", None),
    )
    out_specs = P(EP, "tp")
    return jax.shard_map(
        per_device, mesh=torus, in_specs=in_specs, out_specs=out_specs, check_vma=False
    )
```

profile of v0, /device:TPU:1, one launch (start us, length us, event | category | flops | bytes accessed | tf_op | source)
XLA Modules:
  0.0 214.2 jit_solution(5828575752059299651)
XLA Ops:
  0.0 0.0 copy-start
  0.0 0.8 broadcast_maximum_fusion
  0.8 0.7 broadcast_compare_fusion
  1.5 0.1 reshape.94
  1.6 0.0 copy-done
  1.6 6.0 %gather_fusion = bf16[1024,2048]{1,0:T(8,128)(2,1)} fusion(bf16[128,2048]{1,0:T(8,128)(2,1)S(1)} %copy-done, s32[1024]{0:T(1024)S(1)} %broadcast_clamp_fusion), kind=kCustom, calls=%fused_computation | custom fusion | bytes 8392704 | tf_op jit(solution)/shard_map/jit(_take)/gather | solution.py:62
  7.6 1.1 dynamic-slice_select_fusion
  8.8 10.4 %all_to_all.29 = bf16[16,2,1,32,128]{4,3,0,2,1:T(8,128)(2,1)S(1)} all-to-all(bf16[16,2,1,32,128]{4,3,0,2,1:T(8,128)(2,1)S(1)} %copy.8), channel_id=1, replica_groups=mesh['ep_0'=16,'ep_1'=2,'tp'=16] {'ep_1'}, dimensions={1} | all-to-all | bytes 524288 | tf_op jit(solution)/shard_map/all_to_all | solution.py:26
  19.2 23.4 %all_to_all.30 = bf16[16,2,1,32,128]{4,3,1,2,0:T(8,128)(2,1)S(1)} all-to-all(bf16[16,2,1,32,128]{4,3,1,2,0:T(8,128)(2,1)S(1)} %copy.9), channel_id=1, replica_groups=mesh['ep_0'=16,'ep_1'=2,'tp'=16] {'ep_0'}, dimensions={0} | all-to-all | bytes 524288 | tf_op jit(solution)/shard_map/all_to_all | solution.py:26
  42.6 0.1 copy.10
  42.7 0.5 broadcast_in_dim.31
  43.3 0.0 copy-start.2
  43.3 53.3 %all_to_all.31 = bf16[16,1,1024,128]{2,3,1,0:T(8,128)(2,1)S(1)} all-to-all(bf16[16,1,1024,128]{2,3,1,0:T(8,128)(2,1)S(1)} %broadcast_in_dim.31), channel_id=1, replica_groups=mesh['ep_0'=16,'ep_1'=2,'tp'=16] {'tp'}, dimensions={0} | all-to-all | bytes 8388608 | tf_op jit(solution)/shard_map/all_to_all | solution.py:38
  96.6 0.0 copy-start.1
  96.6 0.0 copy-start.3
  96.6 0.0 copy-start.4
  96.6 1.9 copy-done.1
  98.6 0.0 copy-done.2
  98.6 1.3 fusion.7
  99.8 0.0 copy-done.3
  99.8 0.0 copy-done.4
  99.9 8.5 %convert_bitcast_fusion = bf16[1,128,16,8,128]{4,3,2,1,0:T(8,128)(2,1)} fusion(bf16[1024,2048]{0,1:T(8,128)(2,1)} %bitcast.36, bf16[1,128,2048]{2,1,0:T(8,128)(2,1)S(1)} %copy-done.3, bf16[1,2048,128]{2,1,0:T(8,128)(2,1)S(1)} %copy-done.4, f32[1024,128]{1,0:T(8,128)S(1)} %fusion.7), kind=kOutput, calls=%fused_computation.3 | convolution fusion | flops 1076625408 | bytes 9961472 | tf_op jit(solution)/shard_map/efd,ecf->dec/dot_general | solution.py:71
  108.4 3.3 %copy.15 = bf16[1,128,16,8,128]{4,3,1,0,2:T(8,128)(2,1)S(1)} copy(bf16[1,128,16,8,128]{4,3,2,1,0:T(8,128)(2,1)} %convert_bitcast_fusion) | data formatting | bytes 8388608 | tf_op jit(solution)/shard_map/reshape | solution.py:12
  111.6 47.9 %all_to_all.32 = bf16[16,128,1,1024]{1,3,2,0:T(8,128)(2,1)} all-to-all(bf16[16,128,1,1024]{1,3,2,0:T(8,128)(2,1)S(1)} %bitcast.37), channel_id=1, replica_groups=mesh['ep_0'=16,'ep_1'=2,'tp'=16] {'tp'}, dimensions={0} | all-to-all | bytes 8388608 | tf_op jit(solution)/shard_map/all_to_all | solution.py:50
  159.6 0.0 copy-start.5
  159.6 0.0 copy-start.6
  159.6 3.5 %reduce_sum.12 = bf16[128,1024]{0,1:T(8,128)(2,1)} reduce(bf16[16,128,1,1024]{1,3,2,0:T(8,128)(2,1)} %all_to_all.32, bf16[]{:T(256)} %constant.37.clone.1), dimensions={0,2}, to_apply=%region_0.1 | reduce | flops 1966080 | bytes 4456450 | tf_op jit(solution)/shard_map/reduce_sum | solution.py:51
  163.1 21.3 %all-to-all-start.4 = ((bf16[128,1,32,32]{0,3,1,2:T(8,128)(2,1)}), bf16[128,1,32,32]{0,3,1,2:T(8,128)(2,1)S(1)}, u32[]{:S(2)}, u32[]{:S(2)}) async-start(bf16[128,1,32,32]{0,3,1,2:T(8,128)(2,1)} %bitcast.14), calls=%async_computation.4 | async-start | bytes 524288 | tf_op jit(solution)/shard_map/all_to_all | solution.py:78
  184.5 0.1 reshape.84
  184.5 0.0 copy-done.5
  184.5 0.0 copy-done.6
  184.6 0.1 mul.28
  184.6 22.1 %all-to-all-done.4 = bf16[128,1,32,32]{0,3,1,2:T(8,128)(2,1)S(1)} async-done(((bf16[128,1,32,32]{0,3,1,2:T(8,128)(2,1)}), bf16[128,1,32,32]{0,3,1,2:T(8,128)(2,1)S(1)}, u32[]{:S(2)}, u32[]{:S(2)}) %all-to-all-start.4) | async-done | bytes 262176 | tf_op jit(solution)/shard_map/all_to_all | solution.py:78
  206.7 6.9 %scatter_custom_fusion = f32[128,128]{1,0:T(8,128)S(1)} fusion(s32[1024]{0:T(1024)S(1)} %bitcast.42, bf16[128,1024]{0,1:T(8,128)(2,1)S(1)} %bitcast.40, f32[1024]{0:T(1024)S(1)} %mul.28, f32[]{:T(128)} %constant.11.clone.1), kind=kCustom, calls=%fused_computation.8 | custom fusion | flops 393216 | bytes 331780 | tf_op jit(solution)/shard_map/scatter-add | solution.py:86
  213.6 0.6 convert_element_type.30
  (5 shorter events, 0.1 us)
Async XLA Ops:
  0.0 1.6 copy-start
  43.3 55.3 %copy-start.2 = (bf16[1,2048,128]{2,1,0:T(8,128)(2,1)S(1)}, bf16[1,2048,128]{2,1,0:T(8,128)(2,1)}, u32[]{:S(2)}) copy-start(bf16[1,2048,128]{2,1,0:T(8,128)(2,1)} %param.9) | copy-start | bytes 1572868
  96.6 1.9 copy-start.1
  96.6 3.2 %copy-start.3 = (bf16[1,128,2048]{2,1,0:T(8,128)(2,1)S(1)}, bf16[1,128,2048]{2,1,0:T(8,128)(2,1)}, u32[]{:S(2)}) copy-start(bf16[1,128,2048]{2,1,0:T(8,128)(2,1)} %param.11) | copy-start | bytes 1572868
  96.6 3.2 %copy-start.4 = (bf16[1,2048,128]{2,1,0:T(8,128)(2,1)S(1)}, bf16[1,2048,128]{2,1,0:T(8,128)(2,1)}, u32[]{:S(2)}) copy-start(bf16[1,2048,128]{2,1,0:T(8,128)(2,1)} %param.10) | copy-start | bytes 1572868
  159.6 25.0 %copy-start.5 = (s32[32,32]{1,0:T(8,128)S(1)}, s32[32,32]{1,0:T(8,128)}, u32[]{:S(2)}) copy-start(s32[32,32]{1,0:T(8,128)} %param.7) | copy-start | bytes 12292
  159.6 25.0 %copy-start.6 = (f32[32,32]{1,0:T(8,128)S(1)}, f32[32,32]{1,0:T(8,128)}, u32[]{:S(2)}) copy-start(f32[32,32]{1,0:T(8,128)} %param.8) | copy-start | bytes 12292
  163.1 43.6 %all-to-all-start.4 = ((bf16[128,1,32,32]{0,3,1,2:T(8,128)(2,1)}), bf16[128,1,32,32]{0,3,1,2:T(8,128)(2,1)S(1)}, u32[]{:S(2)}, u32[]{:S(2)}) async-start(bf16[128,1,32,32]{0,3,1,2:T(8,128)(2,1)} %bitcast.14), calls=%async_computation.4 | async-start | bytes 524288 | tf_op jit(solution)/shard_map/all_to_all | solution.py:78
where the time goes:
time: 215 us; the launch traced here: 214 us
  blocking collectives  135 us (63%)
  waiting for transfers between devices  22.1 us (10%)
  starting transfers between devices  21.3 us (10%)
  other arithmetic  13.7 us (6%)
  local copies, waits for them, and re-layouts  12.1 us (6%)
  matrix products  9.8 us (5%)
    all_to_all x1, blocking collectives, sent_to_all(): lax.all_to_all(jnp.broadcast_to(array[None], (peers, *array.shape)), axis...  53.3 us
    all_to_all x1, blocking collectives, summed_on_arrival(): parts = lax.all_to_all(in_blocks(array, dim, peers), axis, 0, 0, tiled=True)  47.9 us
    all_to_all x2, blocking collectives, moved_by_axis(): lax.all_to_all(parts, axes[k], split_axis=k, concat_axis=k, tiled=True)  33.8 us
    all_to_all x1, waiting for transfers between devices, per_device(): lax.all_to_all(summed, EP, split_axis=2, concat_axis=1, tiled=True)  22.1 us
    all_to_all x1, starting transfers between devices, per_device(): lax.all_to_all(summed, EP, split_axis=2, concat_axis=1, tiled=True)  21.3 us
    dot_general x1, matrix products, per_device(): jnp.einsum('efd,ecf->dec', w_down, hidden, preferred_element_type=jnp.flo...  8.52 us
    scatter-add x1, other arithmetic, per_device(): combined = jnp.zeros((local_tokens, feature_cols), jnp.float32).at[clampe...  6.86 us
    gather x1, local copies, waits for them, and re-layouts, per_device(): gathered = jnp.take(tokens, clamped, axis=0)  5.98 us
  transfers between devices with their start and end apart: 1, of which 1 were waited for; matrix products, arithmetic and copies ran while one was open for 0% of the time, Pallas kernels for 0%

commit v1 on v0

--- a/solution.py
+++ b/solution.py
@@ -75,7 +75,9 @@
         0,
     ).astype(jnp.bfloat16)
     summed = summed.reshape(summed.shape[0], experts_here, ep_count, slot_count)
-    returned = lax.all_to_all(summed, EP, split_axis=2, concat_axis=1, tiled=True)
+    returned = jnp.concatenate(
+        lax.all_to_all(jnp.stack(jnp.split(summed, lax.axis_size(EP), axis=2)), EP, 0, 0), axis=1
+    )
     feature_cols = returned.shape[0]
     returned = returned.reshape(feature_cols, experts_here * ep_count * slot_count)
     weights = jnp.where(selected >= 0, affinity, jnp.zeros_like(affinity)).reshape(-1)

time: 215 us -> 233 us (1.084)
  local copies, waits for them, and re-layouts: 12.1 us -> 31.2 us
    unnamed x14 -> x45, local copies, waits for them, and re-layouts: 1.96 us -> 20.4 us
where the time goes in v1:
time: 233 us; the launch traced here: 232 us
  blocking collectives  135 us (58%)
  local copies, waits for them, and re-layouts  31.2 us (13%)
  waiting for transfers between devices  22.1 us (9%)
  starting transfers between devices  21.3 us (9%)
  other arithmetic  12.7 us (5%)
  matrix products  9.8 us (4%)
    all_to_all x1, blocking collectives, sent_to_all(): lax.all_to_all(jnp.broadcast_to(array[None], (peers, *array.shape)), axis...  53.3 us
    all_to_all x1, blocking collectives, summed_on_arrival(): parts = lax.all_to_all(in_blocks(array, dim, peers), axis, 0, 0, tiled=True)  47.9 us
    all_to_all x2, blocking collectives, moved_by_axis(): lax.all_to_all(parts, axes[k], split_axis=k, concat_axis=k, tiled=True)  33.8 us
    all_to_all x1, waiting for transfers between devices, per_device(): lax.all_to_all(jnp.stack(jnp.split(summed, lax.axis_size(EP), axis=2)), E...  22.1 us
    all_to_all x1, starting transfers between devices, per_device(): lax.all_to_all(jnp.stack(jnp.split(summed, lax.axis_size(EP), axis=2)), E...  21.3 us
    unnamed x45, local copies, waits for them, and re-layouts  20.4 us
    dot_general x1, matrix products, per_device(): jnp.einsum('efd,ecf->dec', w_down, hidden, preferred_element_type=jnp.flo...  8.52 us
    scatter-add x1, other arithmetic, per_device(): combined = jnp.zeros((local_tokens, feature_cols), jnp.float32).at[clampe...  6.38 us
  transfers between devices with their start and end apart: 1, of which 1 were waited for; matrix products, arithmetic and copies ran while one was open for 0% of the time, Pallas kernels for 0%

profile of v1, /device:TPU:1, one launch (start us, length us, event | category | flops | bytes accessed | tf_op | source)
XLA Modules:
  0.0 232.3 jit_solution(8446147504871114239)
XLA Ops:
  0.0 0.8 broadcast_compare_fusion
  0.8 0.7 broadcast_maximum_fusion
  1.6 6.0 %gather_fusion = bf16[1024,2048]{1,0:T(8,128)(2,1)} fusion(bf16[128,2048]{1,0:T(8,128)(2,1)S(1)} %copy-done, s32[1024]{0:T(1024)S(1)} %broadcast_clamp_fusion), kind=kCustom, calls=%fused_computation | custom fusion | bytes 8392704 | tf_op jit(solution)/shard_map/jit(_take)/gather | solution.py:62
  7.6 1.1 dynamic-slice_select_fusion
  8.8 10.4 %all_to_all.25 = bf16[16,2,1,32,128]{4,3,0,2,1:T(8,128)(2,1)S(1)} all-to-all(bf16[16,2,1,32,128]{4,3,0,2,1:T(8,128)(2,1)S(1)} %copy.101), channel_id=1, replica_groups=mesh['ep_0'=16,'ep_1'=2,'tp'=16] {'ep_1'}, dimensions={1} | all-to-all | bytes 524288 | tf_op jit(solution)/shard_map/all_to_all | solution.py:26
  19.2 23.4 %all_to_all.26 = bf16[16,2,1,32,128]{4,3,1,2,0:T(8,128)(2,1)S(1)} all-to-all(bf16[16,2,1,32,128]{4,3,1,2,0:T(8,128)(2,1)S(1)} %copy.102), channel_id=1, replica_groups=mesh['ep_0'=16,'ep_1'=2,'tp'=16] {'ep_0'}, dimensions={0} | all-to-all | bytes 524288 | tf_op jit(solution)/shard_map/all_to_all | solution.py:26
  43.3 53.3 %all_to_all.27 = bf16[16,1,1024,128]{2,3,1,0:T(8,128)(2,1)S(1)} all-to-all(bf16[16,1,1024,128]{2,3,1,0:T(8,128)(2,1)S(1)} %broadcast_in_dim.31), channel_id=1, replica_groups=mesh['ep_0'=16,'ep_1'=2,'tp'=16] {'tp'}, dimensions={0} | all-to-all | bytes 8388608 | tf_op jit(solution)/shard_map/all_to_all | solution.py:38
  96.6 1.9 copy-done.1
  98.6 1.3 fusion.6
  99.9 8.5 %convert_bitcast_fusion = bf16[1,128,16,8,128]{4,3,2,1,0:T(8,128)(2,1)} fusion(bf16[1024,2048]{0,1:T(8,128)(2,1)} %bitcast.166, bf16[1,128,2048]{2,1,0:T(8,128)(2,1)S(1)} %copy-done.3, bf16[1,2048,128]{2,1,0:T(8,128)(2,1)S(1)} %copy-done.4, f32[1024,128]{1,0:T(8,128)S(1)} %fusion.6), kind=kOutput, calls=%fused_computation.3 | convolution fusion | flops 1076625408 | bytes 9961472 | tf_op jit(solution)/shard_map/efd,ecf->dec/dot_general | solution.py:71
  108.4 3.3 %copy.108 = bf16[1,128,16,8,128]{4,3,1,0,2:T(8,128)(2,1)S(1)} copy(bf16[1,128,16,8,128]{4,3,2,1,0:T(8,128)(2,1)} %convert_bitcast_fusion) | data formatting | bytes 8388608 | tf_op jit(solution)/shard_map/reshape | solution.py:12
  111.6 47.9 %all_to_all.28 = bf16[16,128,1,1024]{1,3,2,0:T(8,128)(2,1)} all-to-all(bf16[16,128,1,1024]{1,3,2,0:T(8,128)(2,1)S(1)} %bitcast.167), channel_id=1, replica_groups=mesh['ep_0'=16,'ep_1'=2,'tp'=16] {'tp'}, dimensions={0} | all-to-all | bytes 8388608 | tf_op jit(solution)/shard_map/all_to_all | solution.py:50
  159.6 2.9 %reduce_sum.12 = bf16[128,1024]{0,1:T(8,128)(2,1)S(1)} reduce(bf16[16,128,1,1024]{1,3,2,0:T(8,128)(2,1)} %all_to_all.28, bf16[]{:T(256)} %constant.37.clone.1), dimensions={0,2}, to_apply=%region_0.1 | reduce | flops 1966080 | bytes 4456450 | tf_op jit(solution)/shard_map/reduce_sum | solution.py:51
  162.5 0.6 constant_dynamic-update-slice_fusion.31
  163.1 0.6 constant_dynamic-update-slice_fusion.30
  163.6 0.6 constant_dynamic-update-slice_fusion.29
  164.2 0.6 constant_dynamic-update-slice_fusion.28
  164.8 0.6 constant_dynamic-update-slice_fusion.27
  165.4 0.6 constant_dynamic-update-slice_fusion.26
  166.0 0.6 constant_dynamic-update-slice_fusion.25
  166.6 0.6 constant_dynamic-update-slice_fusion.24
  167.2 0.6 constant_dynamic-update-slice_fusion.23
  167.8 0.6 constant_dynamic-update-slice_fusion.22
  168.4 0.6 constant_dynamic-update-slice_fusion.21
  169.0 0.6 constant_dynamic-update-slice_fusion.20
  169.6 0.6 constant_dynamic-update-slice_fusion.19
  170.2 0.6 constant_dynamic-update-slice_fusion.18
  170.8 0.6 constant_dynamic-update-slice_fusion.17
  171.4 0.6 constant_dynamic-update-slice_fusion.16
  172.0 0.6 constant_dynamic-update-slice_fusion.15
  172.6 0.6 constant_dynamic-update-slice_fusion.14
  173.2 0.6 constant_dynamic-update-slice_fusion.13
  173.8 0.6 constant_dynamic-update-slice_fusion.12
  174.4 0.6 constant_dynamic-update-slice_fusion.11
  175.0 0.6 constant_dynamic-update-slice_fusion.10
  175.6 0.6 constant_dynamic-update-slice_fusion.9
  176.2 0.6 constant_dynamic-update-slice_fusion.8
  176.8 0.6 constant_dynamic-update-slice_fusion.7
  177.3 0.6 constant_dynamic-update-slice_fusion.6
  177.9 0.6 constant_dynamic-update-slice_fusion.5
  179.1 0.6 constant_dynamic-update-slice_fusion.3
  179.7 0.6 constant_dynamic-update-slice_fusion.2
  180.3 0.6 constant_dynamic-update-slice_fusion.1
  180.9 0.6 constant_dynamic-update-slice_fusion
  181.5 21.3 %all-to-all-start.4 = ((bf16[32,128,1,1,32]{1,4,3,2,0:T(8,128)(2,1)}), bf16[32,128,1,1,32]{1,4,3,2,0:T(8,128)(2,1)S(1)}, u32[]{:S(2)}, u32[]{:S(2)}) async-start(bf16[32,128,1,1,32]{1,4,3,2,0:T(8,128)(2,1)} %constant_dynamic-update-slice_fusion), calls=%async_computation.4 | async-start | bytes 524288 | tf_op jit(solution)/shard_map/all_to_all | solution.py:79
  203.0 22.1 %all-to-all-done.4 = bf16[32,128,1,1,32]{1,4,3,2,0:T(8,128)(2,1)S(1)} async-done(((bf16[32,128,1,1,32]{1,4,3,2,0:T(8,128)(2,1)}), bf16[32,128,1,1,32]{1,4,3,2,0:T(8,128)(2,1)S(1)}, u32[]{:S(2)}, u32[]{:S(2)}) %all-to-all-start.4) | async-done | bytes 262176 | tf_op jit(solution)/shard_map/all_to_all | solution.py:79
  225.3 6.4 %scatter_custom_fusion = f32[128,128]{1,0:T(8,128)S(1)} fusion(s32[1024]{0:T(1024)S(1)} %bitcast.203, f32[128,1024]{0,1:T(8,128)S(1)} %bitcast_multiply_fusion, f32[]{:T(128)} %constant.11.clone.1), kind=kCustom, calls=%fused_computation.7 | custom fusion | flops 131072 | bytes 589828 | tf_op jit(solution)/shard_map/scatter-add | solution.py:88
  231.7 0.6 convert_element_type.34
  (25 shorter events, 1.8 us)
Async XLA Ops:
  0.0 1.6 copy-start
  43.3 55.3 %copy-start.2 = (bf16[1,2048,128]{2,1,0:T(8,128)(2,1)S(1)}, bf16[1,2048,128]{2,1,0:T(8,128)(2,1)}, u32[]{:S(2)}) copy-start(bf16[1,2048,128]{2,1,0:T(8,128)(2,1)} %param.9) | copy-start | bytes 1572868
  96.6 1.9 copy-start.1
  96.6 3.2 %copy-start.3 = (bf16[1,128,2048]{2,1,0:T(8,128)(2,1)S(1)}, bf16[1,128,2048]{2,1,0:T(8,128)(2,1)}, u32[]{:S(2)}) copy-start(bf16[1,128,2048]{2,1,0:T(8,128)(2,1)} %param.11) | copy-start | bytes 1572868
  96.6 3.2 %copy-start.4 = (bf16[1,2048,128]{2,1,0:T(8,128)(2,1)S(1)}, bf16[1,2048,128]{2,1,0:T(8,128)(2,1)}, u32[]{:S(2)}) copy-start(bf16[1,2048,128]{2,1,0:T(8,128)(2,1)} %param.10) | copy-start | bytes 1572868
  159.6 43.4 %copy-start.5 = (s32[32,32]{1,0:T(8,128)S(1)}, s32[32,32]{1,0:T(8,128)}, u32[]{:S(2)}) copy-start(s32[32,32]{1,0:T(8,128)} %param.7) | copy-start | bytes 12292
  159.6 43.4 %copy-start.6 = (f32[32,32]{1,0:T(8,128)S(1)}, f32[32,32]{1,0:T(8,128)}, u32[]{:S(2)}) copy-start(f32[32,32]{1,0:T(8,128)} %param.8) | copy-start | bytes 12292
  181.5 43.6 %all-to-all-start.4 = ((bf16[32,128,1,1,32]{1,4,3,2,0:T(8,128)(2,1)}), bf16[32,128,1,1,32]{1,4,3,2,0:T(8,128)(2,1)S(1)}, u32[]{:S(2)}, u32[]{:S(2)}) async-start(bf16[32,128,1,1,32]{1,4,3,2,0:T(8,128)(2,1)} %constant_dynamic-update-slice_fusion), calls=%async_computation.4 | async-start | bytes 524288 | tf_op jit(solution)/shard_map/all_to_all | solution.py:79
